TPU v7x, 32 devices: a whole 2x2x4 slice. The times are simulated.
32 devices in a mesh: grp: 2 (over x), ep: 16 (over z, y, core).
Axes of the slice: x: 2, y: 2, z: 4, core: 2. Of those that a mesh axis runs over, the one named last changes fastest.
Arguments:
- tokens: bfloat16 [128, 2048], P(('grp', 'ep')), parts along dimension 0, may hold values from -6 to 6
- lengths: int32 [128], P(('grp', 'ep')), parts along dimension 0, may hold values from 128 to 1024, as said below
- cache_key: bfloat16 [128, 1024, 256], P(('grp', 'ep')), parts along dimension 0, may hold values from -6 to 6
- cache_value: bfloat16 [128, 1024, 256], P(('grp', 'ep')), parts along dimension 0, may hold values from -6 to 6
- routes: int32 [128, 2], P(('grp', 'ep')), parts along dimension 0, may hold values from 0 to 3, all different within a row
- route_logits: float32 [128, 2], P(('grp', 'ep')), parts along dimension 0, may hold values from -6 to 6
- mix_gain: float32 [2048], replicated, may hold values from 0.1 to 1.9
- query_gain: float32 [64], replicated, may hold values from 0.1 to 1.9
- key_gain: float32 [64], replicated, may hold values from 0.1 to 1.9
- head_bias: float32 [16], replicated, may hold values from -9 to -3.5
- w_query: bfloat16 [2048, 1024], P('ep'), may hold values from -0.125 to 0.125
- w_key: bfloat16 [2048, 256], P('ep'), may hold values from -0.125 to 0.125
- w_value: bfloat16 [2048, 256], P('ep'), may hold values from -0.125 to 0.125
- w_out: bfloat16 [1024, 2048], P(None, 'ep'), may hold values from -0.1875 to 0.1875
- ffn_gain: float32 [2048], replicated, may hold values from 0.1 to 1.9
- w_gate: bfloat16 [2048, 28672], P(None, 'ep'), may hold values from -0.125 to 0.125
- w_up: bfloat16 [2048, 28672], P(None, 'ep'), may hold values from -0.125 to 0.125
- w_down: bfloat16 [28672, 2048], P('ep'), may hold values from -0.0625 to 0.0625
Outputs:
- output: bfloat16 [128, 2048], P(('grp', 'ep')), parts along dimension 0
- new_key: bfloat16 [128, 256], P(('grp', 'ep')), parts along dimension 0
- new_value: bfloat16 [128, 256], P(('grp', 'ep')), parts along dimension 0
There are 2 independent parts, one for each index of `grp`. A program takes and returns all parts, laid end to end along the dimension named above; an argument that names none is the same for every part. Nothing has to cross between parts.
Inputs may be any that keep to these rules, and one draw needn't show every extreme that they name: `lengths`: some sequence has all 1024 positions live.
All inputs are finite; a program needn't handle non-finite values.
Results may differ from a plain program's by a relative error of at most 0.0085.
Values may be sent and summed in bfloat16 or wider, within the bound.
No kernel may reach another device: no remote copies, remote signals or barrier semaphores. Data moves between devices by JAX's collectives and lax.ppermute only.
A program may use at most 128 MiB of HBM per device.

v0:
```python
import jax
import jax.numpy as jnp
from jax import lax
from jax.sharding import PartitionSpec as P

HEADS = 16
KV_HEADS = 4
HEAD_DIM = 64
FF = 7168
EXPERTS = 4
EPSILON = 1e-06


def rms_scaled(values, gain):
    return values * lax.rsqrt(jnp.mean(values * values, axis=-1, keepdims=True) + EPSILON) * gain


def route_weights(routes, route_logits):
    experts_iota = jnp.arange(EXPERTS, dtype=jnp.int32)[None, :]
    first_share = jax.nn.sigmoid(route_logits[:, 0:1] - route_logits[:, 1:2])
    second_share = jax.nn.sigmoid(route_logits[:, 1:2] - route_logits[:, 0:1])
    return jnp.where(routes[:, 0:1] == experts_iota, first_share, 0.0) + jnp.where(
        routes[:, 1:2] == experts_iota, second_share, 0.0
    )


def stick_attend(queries, lengths, cache_key, cache_value, query_gain, head_bias):
    batch_rows = queries.shape[0]
    cache_len = cache_key.shape[1]
    group_size = HEADS // KV_HEADS
    normed_query = rms_scaled(queries.reshape(batch_rows, HEADS, HEAD_DIM), query_gain).astype(
        jnp.bfloat16
    )
    normed_query = normed_query.reshape(batch_rows, KV_HEADS, group_size, HEAD_DIM)
    key_heads = cache_key.reshape(batch_rows, cache_len, KV_HEADS, HEAD_DIM)
    value_heads = cache_value.reshape(batch_rows, cache_len, KV_HEADS, HEAD_DIM)
    scores = jnp.einsum(
        "bkgd,blkd->bkgl", normed_query, key_heads, preferred_element_type=jnp.float32
    ) * HEAD_DIM ** (-0.5)
    scores = scores + head_bias.reshape(KV_HEADS, group_size)[None, :, :, None]
    live_mask = (
        jnp.arange(cache_len, dtype=jnp.int32)[None, None, None, :] < lengths[:, None, None, None]
    )
    remain = jnp.where(live_mask, jax.nn.log_sigmoid(-scores), 0.0)
    after_sum = lax.cumsum(remain, axis=3, reverse=True) - remain
    weights = jnp.where(live_mask, jnp.exp(jax.nn.log_sigmoid(scores) + after_sum), 0.0).astype(
        jnp.bfloat16
    )
    attended = jnp.einsum(
        "bkgl,blkd->bkgd", weights, value_heads, preferred_element_type=jnp.float32
    )
    return attended.reshape(batch_rows, HEADS * HEAD_DIM).astype(jnp.bfloat16)


def local(
    tokens,
    lengths,
    cache_key,
    cache_value,
    routes,
    route_logits,
    mix_gain,
    query_gain,
    key_gain,
    head_bias,
    w_query,
    w_key,
    w_value,
    w_out,
    ffn_gain,
    w_gate,
    w_up,
    w_down,
):
    token_rows = tokens.shape[0]
    key_width = w_key.shape[1]
    as_float = tokens.astype(jnp.float32)
    normed = rms_scaled(as_float, mix_gain).astype(jnp.bfloat16)
    pieces = (
        lax.all_gather(w_query, "ep", axis=0, tiled=True),
        lax.all_gather(w_key, "ep", axis=0, tiled=True),
        lax.all_gather(w_value, "ep", axis=0, tiled=True),
    )
    queries, fresh_key, fresh_value = tuple(
        (jnp.dot(normed, weight, preferred_element_type=jnp.float32) for weight in pieces)
    )
    new_key = rms_scaled(fresh_key.reshape(token_rows, KV_HEADS, HEAD_DIM), key_gain)
    new_key = new_key.reshape(token_rows, key_width).astype(jnp.bfloat16)
    new_value = fresh_value.astype(jnp.bfloat16)
    attended = stick_attend(queries, lengths, cache_key, cache_value, query_gain, head_bias)
    mixed = as_float + jnp.dot(
        attended,
        lax.all_gather(w_out, "ep", axis=1, tiled=True),
        preferred_element_type=jnp.float32,
    )
    expert_in = rms_scaled(mixed, ffn_gain).astype(jnp.bfloat16)
    every_gate = lax.all_gather(route_weights(routes, route_logits), "ep", axis=0, tiled=True)
    ff_share = w_gate.shape[1]
    my_expert = lax.axis_index("ep") // (FF // ff_share)
    my_gate = lax.dynamic_slice_in_dim(every_gate, my_expert, 1, 1)
    input_rows = lax.all_gather(expert_in, "ep", axis=0, tiled=True)
    gate_value = jnp.dot(input_rows, w_gate, preferred_element_type=jnp.float32)
    up_value = jnp.dot(input_rows, w_up, preferred_element_type=jnp.float32)
    hidden = (jax.nn.silu(gate_value) * up_value * my_gate).astype(jnp.bfloat16)
    expert_sum = lax.psum_scatter(
        jnp.dot(hidden, w_down, preferred_element_type=jnp.float32),
        "ep",
        scatter_dimension=0,
        tiled=True,
    )
    return ((mixed + expert_sum).astype(jnp.bfloat16), new_key, new_value)


def solution(mesh):
    return jax.shard_map(
        local,
        mesh=mesh,
        in_specs=(
            P(("grp", "ep"), None),
            P(("grp", "ep")),
            P(("grp", "ep"), None, None),
            P(("grp", "ep"), None, None),
            P(("grp", "ep"), None),
            P(("grp", "ep"), None),
            P(),
            P(),
            P(),
            P(),
            P("ep", None),
            P("ep", None),
            P("ep", None),
            P(None, "ep"),
            P(),
            P(None, "ep"),
            P(None, "ep"),
            P("ep", None),
        ),
        out_specs=(P(("grp", "ep"), None), P(("grp", "ep"), None), P(("grp", "ep"), None)),
        check_vma=False,
    )
```

profile of v0, /device:TPU:0, one launch (start us, length us, event | category | flops | bytes accessed | tf_op | source)
XLA Modules:
  0.0 323.6 jit_solution(14233699592130676212)
XLA Ops:
  7.2 0.0 copy-start.5
  7.2 0.0 copy-start
  7.2 0.0 all-gather.11.cloned.1.call-start
  7.2 0.7 all-gather.11.cloned.1.call-update
  7.9 0.0 all-gather.7.cloned.1.call-start
  8.0 0.7 all-gather.7.cloned.1.call-update
  8.7 0.0 all-gather.9.cloned.1.call-start
  8.7 0.7 all-gather.9.cloned.1.call-update
  9.4 0.0 all-gather.13.cloned.1.call-start
  9.4 0.5 all-gather.13.cloned.1.call-update
  10.0 0.0 all-reduce.3.cloned.1.call-start
  10.1 0.8 slice_bitcast_fusion.1
  10.8 0.8 divide_bitcast_fusion.1
  11.6 0.1 add_bitcast_fusion
  11.6 23.2 %all-gather.1 = f32[16,4,4]{2,1,0:T(4,128)S(1)} all-gather(f32[1,4,4]{2,1,0:T(4,128)S(1)} %add_bitcast_fusion), channel_id=1, replica_groups=mesh['grp'=2,'ep'=16] {'ep'}, dimensions={0}, use_global_device_ids=true | all-gather | bytes 1088 | tf_op jit(solution)/shard_map/all_gather | solution.py:97
  34.8 0.1 constant_dynamic-slice_fusion
  34.9 0.1 copy.30
  35.0 0.9 fusion.21
  35.9 0.7 iota_compare_fusion
  36.6 0.0 copy-start.2
  36.6 0.0 copy-start.3
  36.6 4.0 %copy.27 = bf16[4,1024,256]{1,2,0:T(8,128)(2,1)} copy(bf16[4,1024,256]{2,1,0:T(8,128)(2,1)} %param.20) | data formatting | bytes 4194304 | tf_op args[2]
  40.6 0.0 copy-done.5
  40.6 0.1 add.85
  40.7 2.6 copy.28
  43.2 0.1 mul.144
  43.3 0.0 copy-done.8
  43.3 0.6 dynamic-slice
  44.6 6.3 %all-gather.11.cloned.1.call-done = bf16[2048,256]{1,0:T(8,128)(2,1)} async-done(((bf16[128,256]{1,0:T(8,128)(2,1)}), bf16[2048,256]{1,0:T(8,128)(2,1)}) %all-gather.11.cloned.1.call-update) | async-done | bytes 1048592 | tf_op jit(solution)/shard_map/all_gather | solution.py:81
  50.8 0.0 copy-done.2
  50.8 1.5 fusion.37
  52.3 0.1 mul.139
  52.4 0.1 reduce_sum.39
  52.5 0.1 mul.140
  52.6 0.1 mul.141
  52.7 49.7 %all-gather.7.cloned.1.call-done = bf16[2048,1024]{1,0:T(8,128)(2,1)} async-done(((bf16[128,1024]{1,0:T(8,128)(2,1)}), bf16[2048,1024]{1,0:T(8,128)(2,1)}) %all-gather.7.cloned.1.call-update) | async-done | bytes 4194320 | tf_op jit(solution)/shard_map/all_gather | solution.py:80
  102.4 2.9 fusion.36
  105.2 0.1 mul.121
  105.3 0.1 reduce_sum.37
  105.4 0.1 rsqrt.37
  105.5 0.1 reshape.101
  105.6 2.2 fusion.15
  107.9 0.1 reshape.103
  108.0 79.2 %reduce-window.6 = f32[4,4,4,8,128]{4,3,2,1,0:T(8,128)S(1)} reduce-window(f32[4,4,4,8,128]{4,3,2,1,0:T(8,128)S(1)} %reshape.103, f32[]{:T(128)} %constant.36.clone.1), window={size=1x1x1x1x128 pad=0_0x0_0x0_0x0_0x0_127}, to_apply=%region_2.0 | reduce-window | flops 8323072 | bytes 524292 | tf_op jit(solution)/shard_map/reduce-window
  187.2 0.2 slice_reduce_fusion
  187.4 2.8 reduce-window.9
  190.2 0.1 slice.27
  190.3 0.1 broadcast_add_fusion
  190.4 0.1 reduce_window_sum.15
  190.6 0.0 copy-start.4
  190.6 0.9 convolution_convert_fusion
  191.5 0.1 convert_element_type.39
  191.6 3.0 multiply_reduce_fusion
  194.6 0.0 copy-done.4
  194.6 0.1 fusion.25
  194.7 19.6 %all-gather = bf16[16,4,2048]{2,1,0:T(4,128)(2,1)S(1)} all-gather(bf16[1,4,2048]{2,1,0:T(4,128)(2,1)S(1)} %fusion.25), channel_id=1, replica_groups=mesh['grp'=2,'ep'=16] {'ep'}, dimensions={0}, use_global_device_ids=true | all-gather | bytes 278528 | tf_op jit(solution)/shard_map/all_gather | solution.py:101
  214.3 0.1 reshape.107
  214.4 4.4 %fusion.38 = f32[64,1792]{1,0:T(8,128)S(1)} fusion(bf16[64,2048]{1,0:T(8,128)(2,1)S(1)} %reshape.107, bf16[2048,1792]{1,0:T(8,128)(2,1)} %param.33), kind=kOutput, calls=%fused_computation.62 | convolution fusion | flops 469762048 | bytes 8060928 | tf_op jit(solution)/shard_map/dot_general | solution.py:102
  218.8 8.7 %fusion.3 = f32[64,2048]{1,0:T(8,128)} fusion(bf16[1792,2048]{1,0:T(8,128)(2,1)} %param.35, bf16[64,2048]{1,0:T(8,128)(2,1)S(1)} %reshape.107, bf16[2048,1792]{1,0:T(8,128)(2,1)} %param.34, f32[64,1792]{1,0:T(8,128)S(1)} %fusion.38, f32[64]{0:T(128)S(1)} %bitcast.34), kind=kOutput, calls=%fused_computation.8 | convolution fusion | flops 940326912 | bytes 15925504 | tf_op jit(solution)/shard_map/dot_general | solution.py:106
  227.5 0.0 all-reduce.3.cloned.1.call-update
  227.5 0.6 multiply_convert_fusion.3
  228.1 2.1 convolution_convert_fusion.1
  230.2 85.5 %all-reduce.3.cloned.1.call-done = f32[64,2048]{1,0:T(8,128)} async-done(((f32[64,2048]{1,0:T(8,128)}), f32[64,2048]{1,0:T(8,128)}) %all-reduce.3.cloned.1.call-update) | async-done | bytes 524304
  315.7 1.5 fusion.24
  (16 shorter events, 0.1 us)
Async XLA Ops:
  7.2 33.4 %copy-start.5 = (f32[16]{0:T(128)S(1)}, f32[16]{0:T(128)}, u32[]{:S(2)}) copy-start(f32[16]{0:T(128)} %param.27) | copy-start | bytes 196
  7.2 33.5 %copy-start = (bf16[4,1024,256]{2,1,0:T(8,128)(2,1)S(1)}, bf16[4,1024,256]{2,1,0:T(8,128)(2,1)}, u32[]{:S(2)}) copy-start(bf16[4,1024,256]{2,1,0:T(8,128)(2,1)} %param.21) | copy-start | bytes 6291460
  7.2 43.6 %all-gather.11.cloned.1.call-start = ((), (), s32[]{:S(2)}) async-start(), calls=%async_computation.2 | async-start | bytes 1114112 | tf_op jit(solution)/shard_map/all_gather | solution.py:81
  7.9 94.5 %all-gather.7.cloned.1.call-start = ((), (), s32[]{:S(2)}) async-start(), calls=%async_computation | async-start | bytes 4456448 | tf_op jit(solution)/shard_map/all_gather | solution.py:80
  8.7 182.9 %all-gather.9.cloned.1.call-start = ((), (), s32[]{:S(2)}) async-start(), calls=%async_computation.1 | async-start | bytes 4456448 | tf_op jit(solution)/shard_map/all_gather | solution.py:93
  9.4 218.7 %all-gather.13.cloned.1.call-start = ((), (), s32[]{:S(2)}) async-start(), calls=%async_computation.3 | async-start | bytes 1114112 | tf_op jit(solution)/shard_map/all_gather | solution.py:82
  10.0 305.7 %all-reduce.3.cloned.1.call-start = ((), (), s32[]{:S(2)}) async-start(), calls=%async_computation.4 | async-start | bytes 1048576
  36.6 6.7 %copy-start.6 = (f32[64]{0:T(128)S(1)}, f32[64]{0:T(128)}, u32[]{:S(2)}) copy-start(f32[64]{0:T(128)} %param.26) | copy-start | bytes 772
  36.6 6.7 %copy-start.8 = (u32[32]{0:T(128)S(1)}, u32[32]{0:T(128)}, u32[]{:S(2)}) copy-start(u32[32]{0:T(128)} %constant.57) | copy-start | bytes 388
  36.6 14.2 %copy-start.2 = (bf16[4,2048]{1,0:T(4,128)(2,1)S(1)}, bf16[4,2048]{1,0:T(4,128)(2,1)}, u32[]{:S(2)}) copy-start(bf16[4,2048]{1,0:T(4,128)(2,1)} %param.18) | copy-start | bytes 49156
  36.6 14.2 %copy-start.3 = (f32[2048]{0:T(1024)S(1)}, f32[2048]{0:T(1024)}, u32[]{:S(2)}) copy-start(f32[2048]{0:T(1024)} %param.24) | copy-start | bytes 24580
  40.7 64.9 %copy-start.7 = (f32[64]{0:T(128)S(1)}, f32[64]{0:T(128)}, u32[]{:S(2)}) copy-start(f32[64]{0:T(128)} %param.25) | copy-start | bytes 772
  52.7 137.9 %copy-start.1 = (bf16[4,1024,256]{1,2,0:T(8,128)(2,1)S(1)}, bf16[4,1024,256]{1,2,0:T(8,128)(2,1)}, u32[]{:S(2)}) copy-start(bf16[4,1024,256]{1,2,0:T(8,128)(2,1)} %copy.28) | copy-start | bytes 6291460
  190.6 4.1 %copy-start.4 = (f32[2048]{0:T(1024)S(1)}, f32[2048]{0:T(1024)}, u32[]{:S(2)}) copy-start(f32[2048]{0:T(1024)} %param.32) | copy-start | bytes 24580
Sparse Core Ops, SparseCore 0:
  10.2 40.6 all-gather.10
  53.0 49.3 all-gather.6
  104.5 50.9 all-gather.8
  157.6 36.2 all-gather.12
  227.7 87.9 all-reduce.2
where the time goes:
time: 324 us
  waiting for transfers between devices  144 us (44%)
  other arithmetic  87 us (27%)
  blocking collectives  42.8 us (13%)
  matrix products  25.7 us (8%)
  between operations  14.6 us (5%)
  local copies, waits for them, and re-layouts  9.35 us (3%)
    unnamed x6, waiting for transfers between devices  88 us
    another operation x2, other arithmetic  82.1 us
    all_gather x1, waiting for transfers between devices, local(): lax.all_gather(w_query, 'ep', axis=0, tiled=True)  49.7 us
    all_gather x1, blocking collectives, local(): lax.all_gather(route_weights(routes, route_logits), 'ep', axis=0, tiled=T...  23.2 us
    all_gather x1, blocking collectives, local(): input_rows = lax.all_gather(expert_in, 'ep', axis=0, tiled=True)  19.6 us
    dot_general x1, matrix products, local(): jnp.dot(hidden, w_down, preferred_element_type=jnp.float32)  8.67 us
    unnamed x23, local copies, waits for them, and re-layouts  7.29 us
  transfers between devices with their start and end apart: 5, of which 3 were waited for; matrix products, arithmetic and copies ran while one was open for 37% of the time, Pallas kernels for 0%

commit v1 on v0

--- a/solution.py
+++ b/solution.py
@@ -9,6 +9,31 @@
 FF = 7168
 EXPERTS = 4
 EPSILON = 1e-06
+
+
+def _run_view(x_local, join_dim):
+    x_local = jnp.moveaxis(x_local, 0, join_dim)
+    mixed_arr = x_local.shape
+    return x_local.reshape(
+        *mixed_arr[:join_dim],
+        mixed_arr[join_dim] * mixed_arr[join_dim + 1],
+        *mixed_arr[join_dim + 2 :]
+    )
+
+
+def convert_the_shifts_all(panel, along_axis):
+    local_now, local_next = (lax.axis_size(along_axis), lax.axis_index(along_axis))
+    tile_out, part_next = (panel[None], 1)
+    while part_next < local_now:
+        far_arr = lax.ppermute(
+            tile_out, along_axis, tuple(((i, i ^ part_next) for i in range(local_now)))
+        )
+        reached = local_next & part_next == 0
+        tile_out = jnp.concatenate(
+            [jnp.where(reached, tile_out, far_arr), jnp.where(reached, far_arr, tile_out)]
+        )
+        part_next *= 2
+    return tile_out
 
 
 def rms_scaled(values, gain):
@@ -72,6 +97,10 @@
     w_up,
     w_down,
 ):
+
+    def domain_apply(my_data, local_values, dim_no):
+        return _run_view(convert_the_shifts_all(my_data, local_values), dim_no)
+
     token_rows = tokens.shape[0]
     key_width = w_key.shape[1]
     as_float = tokens.astype(jnp.float32)
@@ -98,7 +127,7 @@
     ff_share = w_gate.shape[1]
     my_expert = lax.axis_index("ep") // (FF // ff_share)
     my_gate = lax.dynamic_slice_in_dim(every_gate, my_expert, 1, 1)
-    input_rows = lax.all_gather(expert_in, "ep", axis=0, tiled=True)
+    input_rows = domain_apply(expert_in, "ep", 0)
     gate_value = jnp.dot(input_rows, w_gate, preferred_element_type=jnp.float32)
     up_value = jnp.dot(input_rows, w_up, preferred_element_type=jnp.float32)
     hidden = (jax.nn.silu(gate_value) * up_value * my_gate).astype(jnp.bfloat16)

time: 324 us -> 304 us (0.938)
  blocking collectives: 42.8 us -> 19 us
  waiting for transfers between devices: 144 us -> 148 us
    all_gather x1 -> x0, blocking collectives: 19.6 us -> none  [local(): input_rows = lax.all_gather(expert_in, 'ep', axis=0, tiled=True)]
    ppermute x0 -> x4, waiting for transfers between devices: none -> 14.3 us  [convert_the_shifts_all(): lax.ppermute(tile_out, along_axis, tuple(((i, i ^ part_next) for i in ran...]
    all_gather x1, waiting for transfers between devices: 6.25 us -> 0.02 us  [local(): lax.all_gather(w_key, 'ep', axis=0, tiled=True)]
    all_gather x1, waiting for transfers between devices: 49.7 us -> 45 us  [local(): lax.all_gather(w_query, 'ep', axis=0, tiled=True)]
    all_gather x1, blocking collectives: 23.2 us -> 19 us  [local(): lax.all_gather(route_weights(routes, route_logits), 'ep', axis=0, tiled=T...]
    unnamed x23 -> x26, local copies, waits for them, and re-layouts: 7.29 us -> 7.23 us
  transfers between devices with their start and end apart: 5 -> 9, of which waited for: 3 -> 5; matrix products, arithmetic and copies ran while one was open for 37% -> 39% of each run, Pallas kernels for 0% -> 0%
where the time goes in v1:
time: 304 us
  waiting for transfers between devices  148 us (49%)
  other arithmetic  86.9 us (29%)
  matrix products  25.8 us (8%)
  blocking collectives  19 us (6%)
  between operations  14.7 us (5%)
  local copies, waits for them, and re-layouts  8.6 us (3%)
    unnamed x6, waiting for transfers between devices  88.6 us
    another operation x2, other arithmetic  82.1 us
    all_gather x1, waiting for transfers between devices, local(): lax.all_gather(w_query, 'ep', axis=0, tiled=True)  45 us
    all_gather x1, blocking collectives, local(): lax.all_gather(route_weights(routes, route_logits), 'ep', axis=0, tiled=T...  19 us
    ppermute x4, waiting for transfers between devices, convert_the_shifts_all(): lax.ppermute(tile_out, along_axis, tuple(((i, i ^ part_next) for i in ran...  14.3 us
    dot_general x1, matrix products, local(): jnp.dot(hidden, w_down, preferred_element_type=jnp.float32)  8.68 us
    unnamed x26, local copies, waits for them, and re-layouts  7.23 us
    dot_general x3, matrix products, local(): jnp.dot(normed, weight, preferred_element_type=jnp.float32)  6.47 us
  transfers between devices with their start and end apart: 9, of which 5 were waited for; matrix products, arithmetic and copies ran while one was open for 39% of the time, Pallas kernels for 0%

profile of v1, /device:TPU:0, one launch (start us, length us, event | category | flops | bytes accessed | tf_op | source)
XLA Modules:
  0.0 303.7 jit_solution(370979449245480291)
XLA Ops:
  7.2 0.0 all-gather.6.cloned.1.call-start
  7.2 0.7 all-gather.6.cloned.1.call-update
  7.9 0.0 all-gather.8.cloned.1.call-start
  8.0 0.7 all-gather.8.cloned.1.call-update
  8.7 0.0 all-gather.10.cloned.1.call-start
  8.7 0.7 all-gather.10.cloned.1.call-update
  9.4 0.0 all-gather.12.cloned.1.call-start
  9.4 0.5 all-gather.12.cloned.1.call-update
  10.0 0.0 all-reduce.3.cloned.1.call-start
  10.0 0.8 fusion.21
  10.9 0.7 iota_compare_fusion
  11.7 4.0 %copy.27 = bf16[4,1024,256]{1,2,0:T(8,128)(2,1)} copy(bf16[4,1024,256]{2,1,0:T(8,128)(2,1)} %param.20) | data formatting | bytes 4194304 | tf_op args[2]
  15.6 0.1 add.85
  15.7 2.5 copy.28
  18.3 45.0 %all-gather.6.cloned.1.call-done = bf16[2048,1024]{1,0:T(8,128)(2,1)} async-done(((bf16[128,1024]{1,0:T(8,128)(2,1)}), bf16[2048,1024]{1,0:T(8,128)(2,1)}) %all-gather.6.cloned.1.call-update) | async-done | bytes 4194320 | tf_op jit(solution)/shard_map/all_gather | solution.py:109
  63.3 2.9 fusion.36
  66.2 0.1 mul.121
  66.3 0.1 reduce_sum.37
  66.4 0.1 rsqrt.37
  66.4 0.1 reshape.104
  66.6 2.2 fusion.15
  68.8 0.1 reshape.106
  68.9 79.2 %reduce-window.6 = f32[4,4,4,8,128]{4,3,2,1,0:T(8,128)S(1)} reduce-window(f32[4,4,4,8,128]{4,3,2,1,0:T(8,128)S(1)} %reshape.106, f32[]{:T(128)} %constant.20.clone.1), window={size=1x1x1x1x128 pad=0_0x0_0x0_0x0_0x0_127}, to_apply=%region_2.0 | reduce-window | flops 8323072 | bytes 524292 | tf_op jit(solution)/shard_map/reduce-window
  148.1 0.2 slice_reduce_fusion
  148.3 2.8 reduce-window.9
  151.1 0.1 slice.27
  151.2 0.1 broadcast_add_fusion
  151.4 0.1 reduce_window_sum.15
  151.5 0.9 convolution_convert_fusion
  152.4 0.1 convert_element_type.39
  152.5 3.0 multiply_reduce_fusion
  155.6 0.1 fusion.25
  155.6 0.3 collective-permute-start
  155.9 0.1 add_bitcast_fusion
  156.0 19.0 %all-gather = f32[16,4,4]{2,1,0:T(4,128)S(1)} all-gather(f32[1,4,4]{2,1,0:T(4,128)S(1)} %add_bitcast_fusion), channel_id=1, replica_groups=mesh['grp'=2,'ep'=16] {'ep'}, dimensions={0}, use_global_device_ids=true | all-gather | bytes 1088 | tf_op jit(solution)/shard_map/all_gather | solution.py:126
  175.0 0.1 broadcast_select_fusion.7
  175.1 0.2 collective-permute-start.1
  175.3 0.1 constant_dynamic-slice_fusion
  175.4 0.1 copy.30
  175.5 0.1 mul.144
  175.6 0.6 dynamic-slice
  176.8 2.3 collective-permute-done.1
  179.2 0.1 collective-permute-start.2
  179.3 0.0 all-gather.10.cloned.1.call-done
  179.3 1.5 fusion.37
  180.8 0.1 mul.139
  180.9 0.1 reduce_sum.39
  181.0 3.2 %collective-permute-done.2 = bf16[4,4,2048]{2,1,0:T(4,128)(2,1)S(1)} collective-permute-done((bf16[4,4,2048]{2,1,0:T(4,128)(2,1)S(1)}, bf16[4,4,2048]{2,1,0:T(4,128)(2,1)S(1)}, u32[]{:S(2)}, u32[]{:S(2)}) %collective-permute-start.2) | collective-permute-done | bytes 65568 | tf_op jit(solution)/shard_map/ppermute | solution.py:28
  184.2 0.1 broadcast_select_fusion.3
  184.3 0.1 pad_maximum_fusion.1
  184.4 0.1 collective-permute-start.3
  184.4 0.1 mul.140
  184.5 0.1 mul.141
  184.6 8.8 %collective-permute-done.3 = bf16[8,4,2048]{2,1,0:T(4,128)(2,1)S(1)} collective-permute-done((bf16[8,4,2048]{2,1,0:T(4,128)(2,1)S(1)}, bf16[8,4,2048]{2,1,0:T(4,128)(2,1)S(1)}, u32[]{:S(2)}, u32[]{:S(2)}) %collective-permute-start.3) | collective-permute-done | bytes 131104 | tf_op jit(solution)/shard_map/ppermute | solution.py:28
  193.4 0.1 broadcast_select_fusion.1
  193.6 0.2 pad_maximum_fusion
  193.8 0.1 reshape.109
  193.8 4.5 %fusion.38 = f32[64,1792]{1,0:T(8,128)S(1)} fusion(bf16[64,2048]{1,0:T(8,128)(2,1)S(1)} %reshape.109, bf16[2048,1792]{1,0:T(8,128)(2,1)} %param.33), kind=kOutput, calls=%fused_computation.74 | convolution fusion | flops 469762048 | bytes 8060928 | tf_op jit(solution)/shard_map/dot_general | solution.py:131
  198.3 8.7 %fusion.3 = f32[64,2048]{1,0:T(8,128)} fusion(bf16[1792,2048]{1,0:T(8,128)(2,1)} %param.35, bf16[64,2048]{1,0:T(8,128)(2,1)S(1)} %reshape.109, bf16[2048,1792]{1,0:T(8,128)(2,1)} %param.34, f32[64,1792]{1,0:T(8,128)S(1)} %fusion.38, f32[64]{0:T(128)S(1)} %bitcast.36), kind=kOutput, calls=%fused_computation.8 | convolution fusion | flops 940326912 | bytes 15925504 | tf_op jit(solution)/shard_map/dot_general | solution.py:135
  207.0 0.0 all-reduce.3.cloned.1.call-update
  207.0 0.6 multiply_convert_fusion.3
  207.6 2.1 convolution_convert_fusion.1
  209.7 86.0 %all-reduce.3.cloned.1.call-done = f32[64,2048]{1,0:T(8,128)} async-done(((f32[64,2048]{1,0:T(8,128)}), f32[64,2048]{1,0:T(8,128)}) %all-reduce.3.cloned.1.call-update) | async-done | bytes 524304
  295.7 1.5 fusion.24
  (35 shorter events, 0.2 us)
Async XLA Ops:
  7.2 8.5 %copy-start.7 = (f32[16]{0:T(128)S(1)}, f32[16]{0:T(128)}, u32[]{:S(2)}) copy-start(f32[16]{0:T(128)} %param.27) | copy-start | bytes 196
  7.2 8.5 %copy-start = (bf16[4,1024,256]{2,1,0:T(8,128)(2,1)S(1)}, bf16[4,1024,256]{2,1,0:T(8,128)(2,1)}, u32[]{:S(2)}) copy-start(bf16[4,1024,256]{2,1,0:T(8,128)(2,1)} %param.21) | copy-start | bytes 6291460
  7.2 56.1 %all-gather.6.cloned.1.call-start = ((), (), s32[]{:S(2)}) async-start(), calls=%async_computation | async-start | bytes 4456448 | tf_op jit(solution)/shard_map/all_gather | solution.py:109
  7.9 144.6 %all-gather.8.cloned.1.call-start = ((), (), s32[]{:S(2)}) async-start(), calls=%async_computation.1 | async-start | bytes 4456448 | tf_op jit(solution)/shard_map/all_gather | solution.py:122
  8.7 170.6 %all-gather.10.cloned.1.call-start = ((), (), s32[]{:S(2)}) async-start(), calls=%async_computation.2 | async-start | bytes 1114112 | tf_op jit(solution)/shard_map/all_gather | solution.py:110
  9.4 198.2 %all-gather.12.cloned.1.call-start = ((), (), s32[]{:S(2)}) async-start(), calls=%async_computation.3 | async-start | bytes 1114112 | tf_op jit(solution)/shard_map/all_gather | solution.py:111
  10.0 285.7 %all-reduce.3.cloned.1.call-start = ((), (), s32[]{:S(2)}) async-start(), calls=%async_computation.4 | async-start | bytes 1048576
  11.6 6.6 %copy-start.5 = (s32[4,2]{0,1:T(2,128)S(1)}, s32[4,2]{0,1:T(2,128)}, u32[]{:S(2)}) copy-start(s32[4,2]{0,1:T(2,128)} %param.22) | copy-start | bytes 100
  11.6 6.6 %copy-start.6 = (f32[4,2]{0,1:T(2,128)S(1)}, f32[4,2]{0,1:T(2,128)}, u32[]{:S(2)}) copy-start(f32[4,2]{0,1:T(2,128)} %param.23) | copy-start | bytes 100
  11.6 51.7 %copy-start.2 = (bf16[4,2048]{1,0:T(4,128)(2,1)S(1)}, bf16[4,2048]{1,0:T(4,128)(2,1)}, u32[]{:S(2)}) copy-start(bf16[4,2048]{1,0:T(4,128)(2,1)} %param.18) | copy-start | bytes 49156
  11.6 51.6 %copy-start.3 = (f32[2048]{0:T(1024)S(1)}, f32[2048]{0:T(1024)}, u32[]{:S(2)}) copy-start(f32[2048]{0:T(1024)} %param.24) | copy-start | bytes 24580
  15.7 50.8 %copy-start.9 = (f32[64]{0:T(128)S(1)}, f32[64]{0:T(128)}, u32[]{:S(2)}) copy-start(f32[64]{0:T(128)} %param.25) | copy-start | bytes 772
  18.3 133.2 %copy-start.1 = (bf16[4,1024,256]{1,2,0:T(8,128)(2,1)S(1)}, bf16[4,1024,256]{1,2,0:T(8,128)(2,1)}, u32[]{:S(2)}) copy-start(bf16[4,1024,256]{1,2,0:T(8,128)(2,1)} %copy.28) | copy-start | bytes 6291460
  151.5 4.1 %copy-start.4 = (f32[2048]{0:T(1024)S(1)}, f32[2048]{0:T(1024)}, u32[]{:S(2)}) copy-start(f32[2048]{0:T(1024)} %param.32) | copy-start | bytes 24580
  151.5 24.0 %copy-start.8 = (f32[64]{0:T(128)S(1)}, f32[64]{0:T(128)}, u32[]{:S(2)}) copy-start(f32[64]{0:T(128)} %param.26) | copy-start | bytes 772
  151.5 24.1 %copy-start.10 = (u32[32]{0:T(128)S(1)}, u32[32]{0:T(128)}, u32[]{:S(2)}) copy-start(u32[32]{0:T(128)} %constant.61) | copy-start | bytes 388
  155.6 19.3 %collective-permute-start = (bf16[1,4,2048]{2,1,0:T(4,128)(2,1)S(1)}, bf16[1,4,2048]{2,1,0:T(4,128)(2,1)S(1)}, u32[]{:S(2)}, u32[]{:S(2)}) collective-permute-start(bf16[1,4,2048]{2,1,0:T(4,128)(2,1)S(1)} %fusion.25), channel_id=1, source_target_pairs={{0,1},{1,0},{2,3},{3,2},{4,5},{5,4},{6,7},{7,6},{8,9},{9,8},{10,11... | collective-permute-start | bytes 49160 | tf_op jit(solution)/shard_map/ppermute | solution.py:28
  175.1 4.0 %collective-permute-start.1 = (bf16[2,4,2048]{2,1,0:T(4,128)(2,1)S(1)}, bf16[2,4,2048]{2,1,0:T(4,128)(2,1)S(1)}, u32[]{:S(2)}, u32[]{:S(2)}) collective-permute-start(bf16[2,4,2048]{2,1,0:T(4,128)(2,1)S(1)} %pad_maximum_fusion.3), channel_id=1, source_target_pairs={{0,2},{1,3},{2,0},{3,1},{4,6},{5,7},{6,4},{7,5},{8,10},{9,11},{10,... | collective-permute-start | bytes 98312 | tf_op jit(solution)/shard_map/ppermute | solution.py:28
  179.2 5.0 %collective-permute-start.2 = (bf16[4,4,2048]{2,1,0:T(4,128)(2,1)S(1)}, bf16[4,4,2048]{2,1,0:T(4,128)(2,1)S(1)}, u32[]{:S(2)}, u32[]{:S(2)}) collective-permute-start(bf16[4,4,2048]{2,1,0:T(4,128)(2,1)S(1)} %pad_maximum_fusion.2), channel_id=1, source_target_pairs={{0,4},{1,5},{2,6},{3,7},{4,0},{5,1},{6,2},{7,3},{8,12},{9,13},{10,... | collective-permute-start | bytes 196616 | tf_op jit(solution)/shard_map/ppermute | solution.py:28
  184.4 9.1 %collective-permute-start.3 = (bf16[8,4,2048]{2,1,0:T(4,128)(2,1)S(1)}, bf16[8,4,2048]{2,1,0:T(4,128)(2,1)S(1)}, u32[]{:S(2)}, u32[]{:S(2)}) collective-permute-start(bf16[8,4,2048]{2,1,0:T(4,128)(2,1)S(1)} %pad_maximum_fusion.1), channel_id=1, source_target_pairs={{0,8},{1,9},{2,10},{3,11},{4,12},{5,13},{6,14},{7,15},{8,0},{9,1},... | collective-permute-start | bytes 393224 | tf_op jit(solution)/shard_map/ppermute | solution.py:28
Sparse Core Ops, SparseCore 0:
  10.2 53.0 all-gather.5
  65.4 50.9 all-gather.7
  118.6 36.2 all-gather.9
  156.9 38.1 all-gather.11
  207.1 88.5 all-reduce.2
